TPU v7x, 256 devices: a whole 4x4x8 slice. The times are simulated.
256 devices in a mesh: sp: 64 (over z, x, core), tp: 4 (over y).
Axes of the slice: x: 4, y: 4, z: 8, core: 2. Of those that a mesh axis runs over, the one named last changes fastest.
Arguments:
- residual: bfloat16 [16384, 2048], P(('sp', 'tp')), may hold values from -6 to 6
- query_wide: bfloat16 [16384, 512], P('sp', 'tp'), may hold values from -8 to 8
- key_wide: bfloat16 [16384, 512], P('sp', 'tp'), may hold values from -8 to 8
- value_wide: bfloat16 [16384, 512], P('sp', 'tp'), may hold values from -6 to 6
- query_narrow: bfloat16 [16384, 512], P('sp', 'tp'), may hold values from -8 to 8
- key_narrow: bfloat16 [16384, 512], P('sp', 'tp'), may hold values from -8 to 8
- value_narrow: bfloat16 [16384, 512], P('sp', 'tp'), may hold values from -6 to 6
- gate_wide: float32 [16384, 4], P('sp', 'tp'), may hold values from -2 to 20
- gate_narrow: float32 [16384, 8], P('sp', 'tp'), may hold values from -2 to 20
- out_wide: bfloat16 [512, 2048], replicated, may hold values from -0.1875 to 0.1875
- out_narrow: bfloat16 [512, 2048], replicated, may hold values from -0.1875 to 0.1875
- norm_gain: float32 [2048], replicated, may hold values from 0.1 to 1.9
- routing: int32 [16384, 2], P(('sp', 'tp')), may hold values from 0 to 63, as said below
- route_weight: float32 [16384, 2], P(('sp', 'tp')), may hold values from 0.3 to 1.5
- gate_weight: bfloat16 [64, 2048, 1024], P('sp', None, 'tp'), may hold values from -0.125 to 0.125
- up_weight: bfloat16 [64, 2048, 1024], P('sp', None, 'tp'), may hold values from -0.125 to 0.125
- down_weight: bfloat16 [64, 1024, 2048], P('sp', 'tp'), may hold values from -0.1875 to 0.1875
Outputs:
- result: bfloat16 [16384, 2048], P(('sp', 'tp'))
Inputs may be any that keep to these rules, and one draw needn't show every extreme that they name: `routing`: each row names 2 different experts of one group (experts g * 16 to g * 16 + 15). In each aligned block of 64 rows (the rows of one device) no expert is named by more than 4 rows; one group, the same for all blocks, has each of its experts named by exactly 4 rows of every block.
All inputs are finite; a program needn't handle non-finite values.
Results may differ from a plain program's by a relative error of at most 0.017.
Values may be sent and summed in bfloat16 or wider, within the bound.
A program may use at most 128 MiB of HBM per device.

v0:
```python
import math
import jax
import jax.numpy as jnp
from jax import lax
from jax.sharding import PartitionSpec as P

HW = 128
HN = 64
GROUPS = 4
epsilon = 1e-06


def sent_together(arrays, axis, dim, along):
    both = jnp.concatenate(arrays, axis=along)
    whole, at, outs = (lax.all_gather(both, axis, axis=dim, tiled=True), 0, [])
    for a in arrays:
        outs.append(lax.slice_in_dim(whole, at, at + a.shape[along], axis=along))
        at += a.shape[along]
    return tuple(outs)


def globalize(pieces, shard_rows):
    shards = pieces.shape[0] // shard_rows
    grid = pieces.reshape(shards, shard_rows, pieces.shape[1])
    endings = grid[:, -1, :]
    offsets = jnp.cumsum(endings, axis=0) - endings
    return (grid + offsets[:, None, :]).reshape(pieces.shape)


def head_block(
    state, queries, query_decay, keys, values, key_decay, first_key, first_query, head_width
):
    highest_old, weight_sum, weighted = state
    query_rows = queries.shape[0]
    head_count = query_decay.shape[1]
    key_rows = keys.shape[0]
    grid_query = queries.reshape(query_rows, head_count, head_width)
    grid_key = keys.reshape(key_rows, head_count, head_width)
    grid_value = values.reshape(key_rows, head_count, head_width)
    scores = jnp.einsum("thd,phd->htp", grid_query, grid_key, preferred_element_type=jnp.float32)
    scores = scores * head_width ** (-0.5) + query_decay.T[:, :, None] - key_decay.T[:, None, :]
    query_place = first_query + jnp.arange(query_rows, dtype=jnp.int32)
    key_place = first_key + jnp.arange(key_rows, dtype=jnp.int32)
    scores = jnp.where(key_place[None, None, :] <= query_place[None, :, None], scores, -jnp.inf)
    highest = jnp.maximum(highest_old, jnp.max(scores, axis=2))
    weights = jnp.exp(scores - highest[:, :, None])
    shrink = jnp.exp(highest_old - highest)
    weight_sum = weight_sum * shrink + jnp.sum(weights, axis=2)
    product = jnp.einsum(
        "htp,phd->htd", weights.astype(jnp.bfloat16), grid_value, preferred_element_type=jnp.float32
    )
    weighted = weighted * shrink[:, :, None] + product
    return (highest, weight_sum, weighted)


def fresh_state(head_count, shard_rows, head_width):
    return (
        jnp.full((head_count, shard_rows), -1e30, jnp.float32),
        jnp.zeros((head_count, shard_rows), jnp.float32),
        jnp.zeros((head_count, shard_rows, head_width), jnp.float32),
    )


def finish(state, shard_rows):
    highest, weight_sum, weighted = state
    mixed_heads = weighted / weight_sum[:, :, None]
    joined = jnp.transpose(mixed_heads, (1, 0, 2))
    return joined.reshape(shard_rows, weighted.shape[0] * weighted.shape[2]).astype(jnp.bfloat16)


def body(
    residual,
    query_wide,
    key_wide,
    value_wide,
    query_narrow,
    key_narrow,
    value_narrow,
    gate_wide,
    gate_narrow,
    out_wide,
    out_narrow,
    norm_gain,
    routing,
    route_weight,
    gate_weight,
    up_weight,
    down_weight,
):
    shard_rows = query_wide.shape[0]
    half_rows = shard_rows // 2
    sp_place = lax.axis_index("sp")
    first_query = sp_place * shard_rows
    running_wide = jnp.cumsum(jax.nn.log_sigmoid(gate_wide), axis=0)
    running_narrow = jnp.cumsum(jax.nn.log_sigmoid(gate_narrow), axis=0)
    pieces_wide, pieces_narrow = sent_together((running_wide, running_narrow), "sp", 0, 1)
    every_wide = globalize(pieces_wide, shard_rows)
    every_narrow = globalize(pieces_narrow, shard_rows)
    late_first = first_query + half_rows
    halves = []
    for place, part_wide, part_narrow in (
        (first_query, query_wide[:half_rows], query_narrow[:half_rows]),
        (late_first, query_wide[half_rows:], query_narrow[half_rows:]),
    ):
        halves.append(
            (
                place,
                part_wide,
                part_narrow,
                lax.dynamic_slice_in_dim(every_wide, place, half_rows, 0),
                lax.dynamic_slice_in_dim(every_narrow, place, half_rows, 0),
            )
        )

    def half_state():
        return (
            fresh_state(gate_wide.shape[1], half_rows, HW),
            fresh_state(gate_narrow.shape[1], half_rows, HN),
        )

    state = (half_state(), half_state())
    keys_wide, values_wide, keys_narrow, values_narrow = sent_together(
        (key_wide, value_wide, key_narrow, value_narrow), "sp", 0, 1
    )
    span_rows = keys_wide.shape[0]
    block_size = math.gcd(span_rows, 2048)

    def visit(carried, position):
        inside = position * block_size

        def take_block(source):
            return lax.dynamic_slice_in_dim(source, inside, block_size, 0)

        def take_decay(source):
            return lax.dynamic_slice_in_dim(source, inside, block_size, 0)

        block_kw = take_block(keys_wide)
        block_vw = take_block(values_wide)
        block_kn = take_block(keys_narrow)
        block_vn = take_block(values_narrow)
        block_dw = take_decay(every_wide)
        block_dn = take_decay(every_narrow)

        def one_half(current, half):
            place, part_wide, part_narrow, query_decay_wide, query_decay_narrow = half

            def work(inner):
                first = head_block(
                    inner[0],
                    part_wide,
                    query_decay_wide,
                    block_kw,
                    block_vw,
                    block_dw,
                    inside,
                    place,
                    HW,
                )
                second = head_block(
                    inner[1],
                    part_narrow,
                    query_decay_narrow,
                    block_kn,
                    block_vn,
                    block_dn,
                    inside,
                    place,
                    HN,
                )
                return (first, second)

            def skip(inner):
                return inner

            return lax.cond(inside <= place + half_rows - 1, work, skip, current)

        updated = (one_half(carried[0], halves[0]), one_half(carried[1], halves[1]))
        return (updated, None)

    state, _ = lax.scan(visit, state, jnp.arange(span_rows // block_size, dtype=jnp.int32))
    att_wide = jnp.concatenate(
        [finish(state[0][0], half_rows), finish(state[1][0], half_rows)], axis=0
    )
    att_narrow = jnp.concatenate(
        [finish(state[0][1], half_rows), finish(state[1][1], half_rows)], axis=0
    )
    own_rows = residual.shape[0]
    heads_wide, heads_narrow = (
        lax.all_to_all(att_wide, "tp", split_axis=0, concat_axis=1, tiled=True),
        lax.all_to_all(att_narrow, "tp", split_axis=0, concat_axis=1, tiled=True),
    )
    mixed = jnp.dot(heads_wide, out_wide, preferred_element_type=jnp.float32)
    mixed = mixed + jnp.dot(heads_narrow, out_narrow, preferred_element_type=jnp.float32)
    middle = (residual.astype(jnp.float32) + mixed).astype(jnp.bfloat16)
    middle_wide = middle.astype(jnp.float32)
    spread = jnp.mean(middle_wide * middle_wide, axis=1, keepdims=True)
    normed = (middle_wide * lax.rsqrt(spread + epsilon) * norm_gain).astype(jnp.bfloat16)
    features = normed.shape[1]
    chosen_count = routing.shape[1]
    expert_count = gate_weight.shape[0] * lax.axis_size("sp")
    capacity = own_rows * GROUPS // expert_count
    flat_routes = routing.reshape(-1)
    matches = (flat_routes[:, None] == jnp.arange(expert_count, dtype=jnp.int32)[None, :]).astype(
        jnp.int32
    )
    ranking = jnp.sum((jnp.cumsum(matches, axis=0) - matches) * matches, axis=1)
    placing = flat_routes * capacity + ranking
    picker = (
        placing[None, :] == jnp.arange(expert_count * capacity, dtype=jnp.int32)[:, None]
    ).astype(jnp.bfloat16)
    picker = jnp.sum(picker.reshape(expert_count * capacity, own_rows, chosen_count), axis=2)
    outgoing = jnp.dot(picker, normed, preferred_element_type=jnp.float32).astype(jnp.bfloat16)
    outgoing = outgoing.reshape(expert_count, capacity, features)
    arrived = lax.all_to_all(outgoing, "sp", split_axis=0, concat_axis=0, tiled=True)
    pooled = lax.all_gather(arrived.reshape(-1, features), "tp", axis=0, tiled=True)
    gate_value = jnp.dot(pooled, gate_weight[0], preferred_element_type=jnp.float32)
    up_value = jnp.dot(pooled, up_weight[0], preferred_element_type=jnp.float32)
    hidden = (jax.nn.silu(gate_value) * up_value).astype(jnp.bfloat16)
    answers = lax.psum_scatter(
        jnp.dot(hidden, down_weight[0], preferred_element_type=jnp.float32).astype(jnp.bfloat16),
        "tp",
        scatter_dimension=0,
        tiled=True,
    )
    returned = lax.all_to_all(
        answers.reshape(expert_count, capacity, features),
        "sp",
        split_axis=0,
        concat_axis=0,
        tiled=True,
    )
    picked = jnp.take(returned.reshape(expert_count * capacity, features), placing, axis=0)
    picked = picked.reshape(own_rows, chosen_count, features).astype(jnp.float32)
    combined = jnp.sum(route_weight[:, :, None] * picked, axis=1)
    return (middle_wide + combined).astype(jnp.bfloat16)


def solution(mesh):
    placed = (
        P(("sp", "tp"), None),
        P("sp", "tp"),
        P("sp", "tp"),
        P("sp", "tp"),
        P("sp", "tp"),
        P("sp", "tp"),
        P("sp", "tp"),
        P("sp", "tp"),
        P("sp", "tp"),
        P(),
        P(),
        P(),
        P(("sp", "tp"), None),
        P(("sp", "tp"), None),
        P("sp", None, "tp"),
        P("sp", None, "tp"),
        P("sp", "tp", None),
    )
    return jax.shard_map(
        body, mesh=mesh, in_specs=placed, out_specs=P(("sp", "tp"), None), check_vma=False
    )
```

profile of v0, /device:TPU:1, one launch (start us, length us, event | category | flops | bytes accessed | tf_op | source)
XLA Modules:
  0.0 530.6 jit_solution(731115562800236567)
XLA Ops:
  18.2 48.7 %all_gather.10 = f32[16384,3]{0,1:T(4,128)S(1)} all-gather(f32[256,3]{0,1:T(4,128)S(1)} %pad_maximum_fusion.3), channel_id=1, replica_groups=mesh['sp'=64,'tp'=4] {'sp'}, dimensions={0}, use_global_device_ids=true | all-gather | bytes 199680 | tf_op jit(solution)/shard_map/all_gather | solution.py:15
  67.1 4.9 copy.106
  73.7 9.2 %reshape.388 = f32[64,256,1]{2,1,0:T(8,128)} reshape(f32[16384]{0:T(1024)S(1)} %slice_reduce_fusion) | data formatting | bytes 131072 | tf_op jit(solution)/shard_map/reshape | solution.py:24
  89.4 32.0 %all-gather.3.cloned.1.call-done = bf16[16384,512]{0,1:T(8,128)(2,1)} async-done(((bf16[256,512]{0,1:T(8,128)(2,1)}), bf16[16384,512]{0,1:T(8,128)(2,1)}) %all-gather.3.cloned.1.call-update) | async-done | bytes 16777232 | tf_op jit(solution)/shard_map/all_gather | solution.py:15
  121.4 12.1 %fusion.72 = (bf16[16384,128]{0,1:T(8,128)(2,1)}, bf16[16384,128]{0,1:T(8,128)(2,1)}, bf16[16384,128]{0,1:T(8,128)(2,1)}, bf16[16384,128]{0,1:T(8,128)(2,1)}) fusion(bf16[16384,512]{0,1:T(8,128)(2,1)} %all-gather.3.cloned.1.call-done), kind=kLoop, calls=%fused_computation.146 | loop fusion | bytes 33554432 | tf_op jit(solution)/shard_map/slice | solution.py:17
  138.6 89.0 %while.35 = (s32[]{:T(128)}, f32[1,128]{1,0:T(1,128)}, f32[1,128]{1,0:T(1,128)}, f32[1,128,128]{2,1,0:T(8,128)S(1)}, f32[2,128]{1,0:T(2,128)}, /*index=5*/f32[2,...) while((s32[]{:T(128)}, f32[1,128]{1,0:T(1,128)}, ...), condition=%wide.region_19.20_spmd, body=%wide.region_6.19_spmd.sunk | while | flops 552212480 | bytes 35769752 | solution.py:180
  143.8 2.1 constant_dynamic-slice_fusion.14
  148.2 5.7 %conditional.4 = ((f32[1,128]{1,0:T(1,128)}, f32[1,128]{1,0:T(1,128)}, f32[1,128,128]{2,1,0:T(8,128)S(1)}, f32[2,128]{1,0:T(2,128)}, f32[2,128]{1,0:T(2,128)}, /*index=5*/f32[2,128,64]{1,2,0:T(8,128)S(1)})) conditional(s32[]{:T(128)} %convert_element_type.151, (f32[1,128]{1,0:T(1,128)}, f32[1,128]{1,0:T(1,128)}, f32[1,128,128]{2,1,0:T(8,128)S(1)}, ...), branch_computations={%region_7.7_spmd, %region_8.12_spmd} | conditional | flops 276106240 | bytes 14714172 | solution.py:175
  153.9 5.6 %conditional.5 = ((f32[1,128]{1,0:T(1,128)}, f32[1,128]{1,0:T(1,128)}, f32[1,128,128]{2,1,0:T(8,128)S(1)}, f32[2,128]{1,0:T(2,128)}, f32[2,128]{1,0:T(2,128)}, /*index=5*/f32[2,128,64]{1,2,0:T(8,128)S(1)})) conditional(s32[]{:T(128)} %convert_element_type.152, (f32[1,128]{1,0:T(1,128)}, f32[1,128]{1,0:T(1,128)}, f32[1,128,128]{2,1,0:T(8,128)S(1)}, ...), branch_computations={%region_13.13_spmd, %region_14.18_spmd} | conditional | flops 276106240 | bytes 14714172 | solution.py:175
  164.7 2.1 constant_dynamic-slice_fusion.14
  223.1 2.1 constant_dynamic-slice_fusion.14
  229.1 4.1 all-to-all-start
  234.6 3.0 all-to-all-done
  237.6 3.3 all-to-all-start.1
  243.2 2.1 all-to-all-done.1
  248.5 115.7 %all_to_all.48 = bf16[64,4,2048]{2,1,0:T(4,128)(2,1)S(1)} all-to-all(bf16[64,4,2048]{2,1,0:T(4,128)(2,1)} %reshape.376), channel_id=1, replica_groups=mesh['sp'=64,'tp'=4] {'sp'}, dimensions={0} | all-to-all | bytes 2097152 | tf_op jit(solution)/shard_map/all_to_all | solution.py:214
  365.3 45.8 %all-gather.5.cloned.1.call-done = bf16[1024,2048]{1,0:T(8,128)(2,1)} async-done(((bf16[256,2048]{1,0:T(8,128)(2,1)}), bf16[1024,2048]{1,0:T(8,128)(2,1)}) %all-gather.5.cloned.1.call-update) | async-done | bytes 4194320 | tf_op jit(solution)/shard_map/all_gather | solution.py:215
  411.1 4.8 fusion.39
  415.9 9.1 %convolution_convert_fusion = bf16[1024,2048]{1,0:T(8,128)(2,1)} fusion(bf16[1024,2048]{1,0:T(8,128)(2,1)} %all-gather.5.cloned.1.call-done, bf16[1,256,2048]{2,1,0:T(8,128)(2,1)S(1)} %copy-done.31, bf16[1,2048,256]{2,1,0:T(8,128)(2,1)} %param.38, f32[1024,256]{1,0:T(8,128)} %fusion.39), kind=kOutput, calls=%fused_computation.63 | convolution fusion | flops 2151153664 | bytes 11534336 | tf_op jit(solution)/shard_map/dot_general | solution.py:220
  425.0 50.0 %reduce-scatter.2.cloned.1.call-done = bf16[256,2048]{1,0:T(8,128)(2,1)} async-done(((bf16[1024,2048]{1,0:T(8,128)(2,1)}), bf16[256,2048]{1,0:T(8,128)(2,1)}) %reduce-scatter.2.cloned.1.call-update) | async-done | bytes 1048592 | tf_op jit(solution)/shard_map/reduce_scatter | solution.py:219
  475.0 2.2 reshape.378
  477.2 10.9 %all-to-all-start.3 = ((bf16[64,4,2048]{2,1,0:T(4,128)(2,1)}), bf16[64,4,2048]{2,1,0:T(4,128)(2,1)}, u32[]{:S(2)}, u32[]{:S(2)}) async-start(bf16[64,4,2048]{2,1,0:T(4,128)(2,1)} %reshape.378), calls=%async_computation.4 | async-start | bytes 2097152 | tf_op jit(solution)/shard_map/all_to_all | solution.py:225
  488.7 27.6 %all-to-all-done.3 = bf16[64,4,2048]{2,1,0:T(4,128)(2,1)} async-done(((bf16[64,4,2048]{2,1,0:T(4,128)(2,1)}), bf16[64,4,2048]{2,1,0:T(4,128)(2,1)}, u32[]{:S(2)}, u32[]{:S(2)}) %all-to-all-start.3) | async-done | bytes 1048608 | tf_op jit(solution)/shard_map/all_to_all | solution.py:225
  520.7 2.5 multiply_reduce_fusion
  (248 shorter events, 116.7 us)
Async XLA Ops:
  6.5 238.8 %copy-start = (bf16[512,2048]{1,0:T(8,128)(2,1)S(1)}, bf16[512,2048]{1,0:T(8,128)(2,1)}, u32[]{:S(2)}) copy-start(bf16[512,2048]{1,0:T(8,128)(2,1)} %param.33) | copy-start | bytes 6291460
  6.5 114.8 %all-gather.3.cloned.1.call-start = ((), (), s32[]{:S(2)}) async-start(), calls=%async_computation.5 | async-start | bytes 17039360 | tf_op jit(solution)/shard_map/all_gather | solution.py:15
  14.3 3.9 copy-start.25
  73.7 13.8 %copy-start.22 = (s32[64,2]{0,1:T(2,128)S(1)}, s32[64,2]{0,1:T(2,128)}, u32[]{:S(2)}) copy-start(s32[64,2]{0,1:T(2,128)} %param.35) | copy-start | bytes 1540
  73.7 15.0 %copy-start.9 = (bf16[256,128]{1,0:T(8,128)(2,1)S(1)}, bf16[256,128]{1,0:T(8,128)(2,1)}, u32[]{:S(2)}) copy-start(bf16[256,128]{1,0:T(8,128)(2,1)} %param.24) | copy-start | bytes 196612
  148.5 2.9 copy-start.1
  148.5 2.9 copy-start.17
  148.5 2.9 copy-start.30
  154.2 2.8 copy-start.2
  154.2 2.8 copy-start.16
  227.6 17.8 %copy-start.5 = (bf16[64,2048]{1,0:T(8,128)(2,1)S(1)}, bf16[64,2048]{1,0:T(8,128)(2,1)}, u32[]{:S(2)}) copy-start(bf16[64,2048]{1,0:T(8,128)(2,1)} %param.23) | copy-start | bytes 786436
  229.1 8.6 %all-to-all-start = ((bf16[4,64,128]{2,1,0:T(8,128)(2,1)}), bf16[4,64,128]{2,1,0:T(8,128)(2,1)S(1)}, u32[]{:S(2)}, u32[]{:S(2)}) async-start(bf16[4,64,128]{2,1,0:T(8,128)(2,1)} %bitcast.37), calls=%async_computation | async-start | bytes 131072 | tf_op jit(solution)/shard_map/all_to_all | solution.py:189
  237.6 7.7 %all-to-all-start.1 = ((bf16[4,64,128]{2,1,0:T(8,128)(2,1)}), bf16[4,64,128]{2,1,0:T(8,128)(2,1)S(1)}, u32[]{:S(2)}, u32[]{:S(2)}) async-start(bf16[4,64,128]{2,1,0:T(8,128)(2,1)} %bitcast.43), calls=%async_computation.1 | async-start | bytes 131072 | tf_op jit(solution)/shard_map/all_to_all | solution.py:190
  240.9 170.2 %all-gather.5.cloned.1.call-start = ((), (), s32[]{:S(2)}) async-start(), calls=%async_computation.6 | async-start | bytes 5242880 | tf_op jit(solution)/shard_map/all_gather | solution.py:215
  243.2 3.6 copy-start.6
  243.2 3.6 copy-start.24
  365.3 50.6 %copy-start.31 = (bf16[1,256,2048]{2,1,0:T(8,128)(2,1)S(1)}, bf16[1,256,2048]{2,1,0:T(8,128)(2,1)}, u32[]{:S(2)}) copy-start(bf16[1,256,2048]{2,1,0:T(8,128)(2,1)} %param.39) | copy-start | bytes 3145732
  365.3 109.7 %reduce-scatter.2.cloned.1.call-start = ((), (), s32[]{:S(2)}) async-start(), calls=%async_computation.7 | async-start | bytes 5242880 | tf_op jit(solution)/shard_map/reduce_scatter | solution.py:219
  425.0 63.2 %copy-start.23 = (s32[64,2]{0,1:T(2,128)S(1)}, s32[64,2]{0,1:T(2,128)}, u32[]{:S(2)}) copy-start(s32[64,2]{0,1:T(2,128)} %param.35) | copy-start | bytes 1540
  425.0 63.4 %copy-start.28 = (f32[64,2]{0,1:T(2,128)S(1)}, f32[64,2]{0,1:T(2,128)}, u32[]{:S(2)}) copy-start(f32[64,2]{0,1:T(2,128)} %param.36) | copy-start | bytes 1540
  425.0 63.5 %copy-start.27 = (pred[64,2]{0,1:T(4,128)(4,1)S(1)}, pred[64,2]{0,1:T(4,128)(4,1)}, u32[]{:S(2)}) copy-start(pred[64,2]{0,1:T(4,128)(4,1)} %get-tuple-element.875) | copy-start | bytes 388
  425.0 63.6 %copy-start.26 = (s32[128]{0:T(128)S(1)}, s32[128]{0:T(128)}, u32[]{:S(2)}) copy-start(s32[128]{0:T(128)} %copy-done.25) | copy-start | bytes 1540
  477.2 39.0 %all-to-all-start.3 = ((bf16[64,4,2048]{2,1,0:T(4,128)(2,1)}), bf16[64,4,2048]{2,1,0:T(4,128)(2,1)}, u32[]{:S(2)}, u32[]{:S(2)}) async-start(bf16[64,4,2048]{2,1,0:T(4,128)(2,1)} %reshape.378), calls=%async_computation.4 | async-start | bytes 2097152 | tf_op jit(solution)/shard_map/all_to_all | solution.py:225
  519.3 4.0 copy-start.4
  (14 other events, 22.4 us)
Sparse Core Ops, SparseCore 0:
  11.3 110.0 all-gather.2
  365.4 45.6 all-gather.4
  425.1 49.8 reduce-scatter.1
where the time goes:
time: 533 us; the launch traced here: 531 us
  blocking collectives  164 us (31%)
  waiting for transfers between devices  161 us (30%)
  local copies, waits for them, and re-layouts  127 us (24%)
  matrix products  23.7 us (4%)
  starting transfers between devices  18.5 us (3%)
  other arithmetic  16.4 us (3%)
  between operations  13.5 us (3%)
  loops' own time  6.28 us (1%)
    all_to_all x1, blocking collectives, body(): lax.all_to_all(outgoing, 'sp', split_axis=0, concat_axis=0, tiled=True)  116 us
    dynamic_slice x32, local copies, waits for them, and re-layouts, take_block(): return lax.dynamic_slice_in_dim(source, inside, block_size, 0)  51.8 us
    reduce_scatter x1, waiting for transfers between devices, body(): lax.psum_scatter(jnp.dot(hidden, down_weight[0], preferred_element_type=j...  50 us
    all_gather x1, blocking collectives, sent_together(): whole, at, outs = (lax.all_gather(both, axis, axis=dim, tiled=True), 0, [])  48.7 us
    all_gather x1, waiting for transfers between devices, body(): lax.all_gather(arrived.reshape(-1, features), 'tp', axis=0, tiled=True)  45.8 us
    all_gather x1, waiting for transfers between devices, sent_together(): whole, at, outs = (lax.all_gather(both, axis, axis=dim, tiled=True), 0, [])  32 us
    all_to_all x1, waiting for transfers between devices, body(): lax.all_to_all(answers.reshape(expert_count, capacity, features), 'sp', s...  27.6 us
    slice x4, local copies, waits for them, and re-layouts, sent_together(): outs.append(lax.slice_in_dim(whole, at, at + a.shape[along], axis=along))  17.3 us
  transfers between devices with their start and end apart: 6, of which 6 were waited for; matrix products, arithmetic and copies ran while one was open for 6% of the time, Pallas kernels for 0%

commit v1 on v0

--- a/solution.py
+++ b/solution.py
@@ -212,7 +212,10 @@
     outgoing = jnp.dot(picker, normed, preferred_element_type=jnp.float32).astype(jnp.bfloat16)
     outgoing = outgoing.reshape(expert_count, capacity, features)
     arrived = lax.all_to_all(outgoing, "sp", split_axis=0, concat_axis=0, tiled=True)
-    pooled = lax.all_gather(arrived.reshape(-1, features), "tp", axis=0, tiled=True)
+    array = arrived.reshape(-1, features)
+    count = lax.axis_size("tp")
+    repeats = [count if d == 0 else 1 for d in range(array.ndim)]
+    pooled = lax.all_to_all(jnp.tile(array, repeats), "tp", split_axis=0, concat_axis=0, tiled=True)
     gate_value = jnp.dot(pooled, gate_weight[0], preferred_element_type=jnp.float32)
     up_value = jnp.dot(pooled, up_weight[0], preferred_element_type=jnp.float32)
     hidden = (jax.nn.silu(gate_value) * up_value).astype(jnp.bfloat16)

time: 533 us -> 535 us (level)
  blocking collectives: 164 us -> 215 us
  waiting for transfers between devices: 161 us -> 110 us
    all_to_all x0 -> x1, blocking collectives: none -> 50.4 us  [body(): lax.all_to_all(jnp.tile(array, repeats), 'tp', split_axis=0, concat_axis=...]
    all_gather x1 -> x0, waiting for transfers between devices: 45.8 us -> none  [body(): lax.all_gather(arrived.reshape(-1, features), 'tp', axis=0, tiled=True)]
  transfers between devices with their start and end apart: 6 -> 5, of which waited for: 6 -> 5; matrix products, arithmetic and copies ran while one was open for 6% -> 6% of each run, Pallas kernels for 0% -> 0%
where the time goes in v1:
time: 535 us; the launch traced here: 533 us
  blocking collectives  215 us (40%)
  local copies, waits for them, and re-layouts  131 us (24%)
  waiting for transfers between devices  110 us (21%)
  matrix products  21.2 us (4%)
  starting transfers between devices  18.4 us (3%)
  other arithmetic  16.9 us (3%)
  between operations  13.8 us (3%)
  loops' own time  6.28 us (1%)
    all_to_all x1, blocking collectives, body(): lax.all_to_all(outgoing, 'sp', split_axis=0, concat_axis=0, tiled=True)  116 us
    dynamic_slice x32, local copies, waits for them, and re-layouts, take_block(): return lax.dynamic_slice_in_dim(source, inside, block_size, 0)  52 us
    all_to_all x1, blocking collectives, body(): lax.all_to_all(jnp.tile(array, repeats), 'tp', split_axis=0, concat_axis=...  50.4 us
    all_gather x1, blocking collectives, sent_together(): whole, at, outs = (lax.all_gather(both, axis, axis=dim, tiled=True), 0, [])  48.7 us
    reduce_scatter x1, waiting for transfers between devices, body(): lax.psum_scatter(jnp.dot(hidden, down_weight[0], preferred_element_type=j...  45.6 us
    all_gather x1, waiting for transfers between devices, sent_together(): whole, at, outs = (lax.all_gather(both, axis, axis=dim, tiled=True), 0, [])  31.6 us
    all_to_all x1, waiting for transfers between devices, body(): lax.all_to_all(answers.reshape(expert_count, capacity, features), 'sp', s...  27.6 us
    slice x4, local copies, waits for them, and re-layouts, sent_together(): outs.append(lax.slice_in_dim(whole, at, at + a.shape[along], axis=along))  17.3 us
  transfers between devices with their start and end apart: 5, of which 5 were waited for; matrix products, arithmetic and copies ran while one was open for 6% of the time, Pallas kernels for 0%

profile of v1, /device:TPU:1, one launch (start us, length us, event | category | flops | bytes accessed | tf_op | source)
XLA Modules:
  0.0 532.9 jit_solution(12834658208189892232)
XLA Ops:
  18.3 48.7 %all_gather.7 = f32[16384,3]{0,1:T(4,128)S(1)} all-gather(f32[256,3]{0,1:T(4,128)S(1)} %pad_maximum_fusion.3), channel_id=1, replica_groups=mesh['sp'=64,'tp'=4] {'sp'}, dimensions={0}, use_global_device_ids=true | all-gather | bytes 199680 | tf_op jit(solution)/shard_map/all_gather | solution.py:15
  67.1 5.0 copy.106
  74.0 9.2 %reshape.391 = f32[64,256,1]{2,1,0:T(8,128)} reshape(f32[16384]{0:T(1024)S(1)} %slice_reduce_fusion) | data formatting | bytes 131072 | tf_op jit(solution)/shard_map/reshape | solution.py:24
  89.9 31.6 %all-gather.2.cloned.1.call-done = bf16[16384,512]{0,1:T(8,128)(2,1)} async-done(((bf16[256,512]{0,1:T(8,128)(2,1)}), bf16[16384,512]{0,1:T(8,128)(2,1)}) %all-gather.2.cloned.1.call-update) | async-done | bytes 16777232 | tf_op jit(solution)/shard_map/all_gather | solution.py:15
  121.5 12.1 %fusion.72 = (bf16[16384,128]{0,1:T(8,128)(2,1)}, bf16[16384,128]{0,1:T(8,128)(2,1)}, bf16[16384,128]{0,1:T(8,128)(2,1)}, bf16[16384,128]{0,1:T(8,128)(2,1)}) fusion(bf16[16384,512]{0,1:T(8,128)(2,1)} %all-gather.2.cloned.1.call-done), kind=kLoop, calls=%fused_computation.146 | loop fusion | bytes 33554432 | tf_op jit(solution)/shard_map/slice | solution.py:17
  138.7 89.9 %while.35 = (s32[]{:T(128)}, f32[1,128]{1,0:T(1,128)}, f32[1,128]{1,0:T(1,128)}, f32[1,128,128]{2,1,0:T(8,128)S(1)}, f32[2,128]{1,0:T(2,128)}, /*index=5*/f32[2,...) while((s32[]{:T(128)}, f32[1,128]{1,0:T(1,128)}, ...), condition=%wide.region_19.20_spmd, body=%wide.region_6.19_spmd.sunk | while | flops 552212480 | bytes 35769752 | solution.py:180
  148.4 5.7 %conditional.4 = ((f32[1,128]{1,0:T(1,128)}, f32[1,128]{1,0:T(1,128)}, f32[1,128,128]{2,1,0:T(8,128)S(1)}, f32[2,128]{1,0:T(2,128)}, f32[2,128]{1,0:T(2,128)}, /*index=5*/f32[2,128,64]{1,2,0:T(8,128)S(1)})) conditional(s32[]{:T(128)} %convert_element_type.151, (f32[1,128]{1,0:T(1,128)}, f32[1,128]{1,0:T(1,128)}, f32[1,128,128]{2,1,0:T(8,128)S(1)}, ...), branch_computations={%region_7.7_spmd, %region_8.12_spmd} | conditional | flops 276106240 | bytes 14714172 | solution.py:175
  154.1 5.7 %conditional.5 = ((f32[1,128]{1,0:T(1,128)}, f32[1,128]{1,0:T(1,128)}, f32[1,128,128]{2,1,0:T(8,128)S(1)}, f32[2,128]{1,0:T(2,128)}, f32[2,128]{1,0:T(2,128)}, /*index=5*/f32[2,128,64]{1,2,0:T(8,128)S(1)})) conditional(s32[]{:T(128)} %convert_element_type.152, (f32[1,128]{1,0:T(1,128)}, f32[1,128]{1,0:T(1,128)}, f32[1,128,128]{2,1,0:T(8,128)S(1)}, ...), branch_computations={%region_13.13_spmd, %region_14.18_spmd} | conditional | flops 276106240 | bytes 14714172 | solution.py:175
  165.1 2.1 constant_dynamic-slice_fusion.14
  174.9 2.1 constant_dynamic-slice_fusion.14
  214.2 2.1 constant_dynamic-slice_fusion.14
  230.0 4.0 all-to-all-start
  235.4 3.0 all-to-all-done
  238.5 3.3 all-to-all-start.1
  244.1 2.1 all-to-all-done.1
  249.4 116.2 %all_to_all.57 = bf16[64,4,2048]{2,1,0:T(4,128)(2,1)} all-to-all(bf16[64,4,2048]{2,1,0:T(4,128)(2,1)} %reshape.380), channel_id=1, replica_groups=mesh['sp'=64,'tp'=4] {'sp'}, dimensions={0} | all-to-all | bytes 2097152 | tf_op jit(solution)/shard_map/all_to_all | solution.py:214
  367.5 50.4 %all_to_all.58 = bf16[4,256,2048]{2,1,0:T(8,128)(2,1)S(1)} all-to-all(bf16[4,256,2048]{2,1,0:T(8,128)(2,1)S(1)} %tile.9), channel_id=1, replica_groups=mesh['sp'=64,'tp'=4] {'tp'}, dimensions={0} | all-to-all | bytes 8388608 | tf_op jit(solution)/shard_map/all_to_all | solution.py:218
  419.9 2.3 fusion.39
  422.2 9.1 %convolution_convert_fusion = bf16[1024,2048]{1,0:T(8,128)(2,1)} fusion(bf16[1024,2048]{1,0:T(8,128)(2,1)} %bitcast.142, bf16[1,256,2048]{2,1,0:T(8,128)(2,1)S(1)} %copy-done.33, bf16[1,2048,256]{2,1,0:T(8,128)(2,1)} %param.38, f32[1024,256]{1,0:T(8,128)} %fusion.39), kind=kOutput, calls=%fused_computation.63 | convolution fusion | flops 2151153664 | bytes 11534336 | tf_op jit(solution)/shard_map/dot_general | solution.py:223
  431.3 45.6 %reduce-scatter.2.cloned.1.call-done = bf16[256,2048]{1,0:T(8,128)(2,1)} async-done(((bf16[1024,2048]{1,0:T(8,128)(2,1)}), bf16[256,2048]{1,0:T(8,128)(2,1)}) %reduce-scatter.2.cloned.1.call-update) | async-done | bytes 1048592 | tf_op jit(solution)/shard_map/reduce_scatter | solution.py:222
  477.0 2.3 reshape.381
  479.2 10.9 %all-to-all-start.4 = ((bf16[64,4,2048]{2,1,0:T(4,128)(2,1)}), bf16[64,4,2048]{2,1,0:T(4,128)(2,1)}, u32[]{:S(2)}, u32[]{:S(2)}) async-start(bf16[64,4,2048]{2,1,0:T(4,128)(2,1)} %reshape.381), calls=%async_computation.5 | async-start | bytes 2097152 | tf_op jit(solution)/shard_map/all_to_all | solution.py:228
  490.7 27.6 %all-to-all-done.4 = bf16[64,4,2048]{2,1,0:T(4,128)(2,1)} async-done(((bf16[64,4,2048]{2,1,0:T(4,128)(2,1)}), bf16[64,4,2048]{2,1,0:T(4,128)(2,1)}, u32[]{:S(2)}, u32[]{:S(2)}) %all-to-all-start.4) | async-done | bytes 1048608 | tf_op jit(solution)/shard_map/all_to_all | solution.py:228
  522.7 2.5 multiply_reduce_fusion
  (251 shorter events, 120.8 us)
Async XLA Ops:
  6.5 239.7 %copy-start = (bf16[512,2048]{1,0:T(8,128)(2,1)S(1)}, bf16[512,2048]{1,0:T(8,128)(2,1)}, u32[]{:S(2)}) copy-start(bf16[512,2048]{1,0:T(8,128)(2,1)} %param.33) | copy-start | bytes 6291460
  6.5 114.9 %all-gather.2.cloned.1.call-start = ((), (), s32[]{:S(2)}) async-start(), calls=%async_computation.6 | async-start | bytes 17039360 | tf_op jit(solution)/shard_map/all_gather | solution.py:15
  14.3 3.9 copy-start.26
  74.0 14.0 %copy-start.23 = (s32[64,2]{0,1:T(2,128)S(1)}, s32[64,2]{0,1:T(2,128)}, u32[]{:S(2)}) copy-start(s32[64,2]{0,1:T(2,128)} %param.35) | copy-start | bytes 1540
  74.0 15.2 %copy-start.10 = (bf16[256,128]{1,0:T(8,128)(2,1)S(1)}, bf16[256,128]{1,0:T(8,128)(2,1)}, u32[]{:S(2)}) copy-start(bf16[256,128]{1,0:T(8,128)(2,1)} %param.24) | copy-start | bytes 196612
  148.7 2.9 copy-start.1
  148.7 2.9 copy-start.18
  148.8 2.8 copy-start.31
  154.4 2.9 copy-start.2
  154.4 2.9 copy-start.17
  154.4 2.9 copy-start.30
  228.5 17.7 %copy-start.6 = (bf16[64,2048]{1,0:T(8,128)(2,1)S(1)}, bf16[64,2048]{1,0:T(8,128)(2,1)}, u32[]{:S(2)}) copy-start(bf16[64,2048]{1,0:T(8,128)(2,1)} %param.23) | copy-start | bytes 786436
  230.0 8.5 %all-to-all-start = ((bf16[4,64,128]{2,1,0:T(8,128)(2,1)}), bf16[4,64,128]{2,1,0:T(8,128)(2,1)S(1)}, u32[]{:S(2)}, u32[]{:S(2)}) async-start(bf16[4,64,128]{2,1,0:T(8,128)(2,1)} %bitcast.37), calls=%async_computation | async-start | bytes 131072 | tf_op jit(solution)/shard_map/all_to_all | solution.py:189
  238.5 7.7 %all-to-all-start.1 = ((bf16[4,64,128]{2,1,0:T(8,128)(2,1)}), bf16[4,64,128]{2,1,0:T(8,128)(2,1)S(1)}, u32[]{:S(2)}, u32[]{:S(2)}) async-start(bf16[4,64,128]{2,1,0:T(8,128)(2,1)} %bitcast.43), calls=%async_computation.1 | async-start | bytes 131072 | tf_op jit(solution)/shard_map/all_to_all | solution.py:190
  241.8 235.2 %reduce-scatter.2.cloned.1.call-start = ((), (), s32[]{:S(2)}) async-start(), calls=%async_computation.7 | async-start | bytes 5242880 | tf_op jit(solution)/shard_map/reduce_scatter | solution.py:222
  244.1 3.6 copy-start.7
  244.1 3.6 copy-start.25
  367.4 52.4 %copy-start.32 = (bf16[1,2048,256]{2,1,0:T(8,128)(2,1)S(1)}, bf16[1,2048,256]{2,1,0:T(8,128)(2,1)}, u32[]{:S(2)}) copy-start(bf16[1,2048,256]{2,1,0:T(8,128)(2,1)} %param.37) | copy-start | bytes 3145732
  431.3 58.9 %copy-start.24 = (s32[64,2]{0,1:T(2,128)S(1)}, s32[64,2]{0,1:T(2,128)}, u32[]{:S(2)}) copy-start(s32[64,2]{0,1:T(2,128)} %param.35) | copy-start | bytes 1540
  431.3 59.1 %copy-start.29 = (f32[64,2]{0,1:T(2,128)S(1)}, f32[64,2]{0,1:T(2,128)}, u32[]{:S(2)}) copy-start(f32[64,2]{0,1:T(2,128)} %param.36) | copy-start | bytes 1540
  431.3 59.2 %copy-start.28 = (pred[64,2]{0,1:T(4,128)(4,1)S(1)}, pred[64,2]{0,1:T(4,128)(4,1)}, u32[]{:S(2)}) copy-start(pred[64,2]{0,1:T(4,128)(4,1)} %get-tuple-element.875) | copy-start | bytes 388
  431.3 59.3 %copy-start.27 = (s32[128]{0:T(128)S(1)}, s32[128]{0:T(128)}, u32[]{:S(2)}) copy-start(s32[128]{0:T(128)} %copy-done.26) | copy-start | bytes 1540
  479.2 39.0 %all-to-all-start.4 = ((bf16[64,4,2048]{2,1,0:T(4,128)(2,1)}), bf16[64,4,2048]{2,1,0:T(4,128)(2,1)}, u32[]{:S(2)}, u32[]{:S(2)}) async-start(bf16[64,4,2048]{2,1,0:T(4,128)(2,1)} %reshape.381), calls=%async_computation.5 | async-start | bytes 2097152 | tf_op jit(solution)/shard_map/all_to_all | solution.py:228
  521.3 4.0 copy-start.4
  (15 other events, 24.1 us)
Sparse Core Ops, SparseCore 0:
  11.3 110.0 all-gather.1
  431.4 45.5 reduce-scatter.1
